TPU v7x, 32 devices: a whole 2x2x4 slice. The times are simulated.
32 devices in a mesh: sp: 4 (over z), fs: 4 (over y, x), tp: 2 (over core).
Axes of the slice: x: 2, y: 2, z: 4, core: 2. Of those that a mesh axis runs over, the one named last changes fastest.
Arguments:
- tokens: bfloat16 [2048, 2048], P(('fs', 'sp')), parts along dimension 0, may hold values from -6 to 6
- norm_gain: bfloat16 [2048], replicated, may hold values from 0.099609375 to 1.8984375
- query_down: bfloat16 [2048, 512], P('sp'), may hold values from -0.125 to 0.125
- query_gain: bfloat16 [512], replicated, may hold values from 0.099609375 to 1.8984375
- latent_down: bfloat16 [2048, 256], replicated, may hold values from -0.125 to 0.125
- latent_gain: bfloat16 [256], replicated, may hold values from 0.099609375 to 1.8984375
- rope_down: bfloat16 [2048, 64], replicated, may hold values from -30 to 30
- query_up: bfloat16 [512, 1536], P(None, 'tp'), may hold values from -0.25 to 0.25
- key_up: bfloat16 [256, 1024], P(None, 'tp'), may hold values from -0.75 to 0.75
- value_up: bfloat16 [256, 1024], P(None, 'tp'), may hold values from -0.375 to 0.375
- glu_value: bfloat16 [2048, 1024], P('sp', 'tp'), may hold values from -0.125 to 0.125
- glu_gate: bfloat16 [2048, 1024], P('sp', 'tp'), may hold values from -0.125 to 0.125
- conv_taps: bfloat16 [31, 1024], P(None, 'tp'), may hold values from -1 to 1
- group_gain: bfloat16 [1024], P('tp'), may hold values from 0.099609375 to 1.8984375
- head_proj: bfloat16 [1024, 2048], P('tp', 'sp'), may hold values from -0.75 to 0.75
- channel_proj: bfloat16 [1024, 2048], P('tp', 'sp'), may hold values from -0.1875 to 0.1875
Outputs:
- mixed_out: bfloat16 [2048, 2048], P(('fs', 'sp'), 'tp'), parts along dimension 0
- log_weight: float32 [8, 2048], P('tp', ('fs', 'sp')), parts along dimension 1
There are 4 independent parts, one for each index of `fs`. A program takes and returns all parts, laid end to end along the dimension named above; an argument that names none is the same for every part. Nothing has to cross between parts.
All inputs are finite; a program needn't handle non-finite values.
Results may differ from a plain program's by a relative error of at most 0.015.
The roundings to bfloat16 on the way count: a program that leaves them out, or rounds other values in their place, can miss the bound.
Values may be sent and summed in bfloat16 or wider, within the bound.
A program may use at most 128 MiB of HBM per device.

v0:
```python
import jax
import jax.numpy as jnp
from jax import lax
from jax.sharding import PartitionSpec as P

NOPE = 128
ROPE = 64
VDIM = 128
KVR = 256
CH = 1024
GROUPS = 8
GRID_W = 64
norm_eps = 1e-06
rope_base = 10000.0
far_below = -1e30


def padded_2(block, sides, width):
    for axis, dim in sides:
        count = lax.axis_size(axis)
        forward = [(i, i + 1) for i in range(count - 1)]
        backward = [(target, source) for source, target in forward]
        low = lax.ppermute(
            lax.slice_in_dim(block, block.shape[dim] - width, None, axis=dim), axis, forward
        )
        high = lax.ppermute(lax.slice_in_dim(block, 0, width, axis=dim), axis, backward)
        block = jnp.concatenate([low, block, high], axis=dim)
    return block


def rms_scale(values, scale_gain):
    inv_rms = lax.rsqrt(jnp.mean(values * values, axis=-1, keepdims=True) + norm_eps)
    return values * inv_rms * scale_gain.astype(jnp.float32)


def angles_for(positions, rope_size):
    quarter = rope_size // 4
    inverse = rope_base ** (-jnp.arange(quarter, dtype=jnp.float32) / quarter)
    grid_row = (positions // GRID_W).astype(jnp.float32)
    grid_col = (positions % GRID_W).astype(jnp.float32)
    return jnp.concatenate([grid_row[:, None] * inverse, grid_col[:, None] * inverse], axis=-1)


def rotate(values, angles):
    half_size = values.shape[-1] // 2
    front_half = values[..., :half_size]
    back_half = values[..., half_size:]
    cosine = jnp.cos(angles)
    sine_part = jnp.sin(angles)
    return jnp.concatenate(
        [front_half * cosine - back_half * sine_part, back_half * cosine + front_half * sine_part],
        axis=-1,
    )


def key_block(normed, latent_down, latent_gain, rope_down, positions):
    latent = jnp.dot(normed, latent_down, preferred_element_type=jnp.float32)
    latent = rms_scale(latent, latent_gain).astype(jnp.bfloat16)
    rope_key = jnp.dot(normed, rope_down, preferred_element_type=jnp.float32)
    rope_key = rotate(rope_key, angles_for(positions, rope_key.shape[-1])).astype(jnp.bfloat16)
    return jnp.concatenate([latent, rope_key], axis=1)


def per_device(
    tokens,
    norm_gain,
    query_down,
    query_gain,
    latent_down,
    latent_gain,
    rope_down,
    query_up,
    key_up,
    value_up,
    glu_value,
    glu_gate,
    conv_taps,
    group_gain,
    head_proj,
    channel_proj,
):
    tok_count = tokens.shape[0]
    reach_rows = conv_taps.shape[0] // 2
    head_count = key_up.shape[1] // NOPE
    normed = rms_scale(tokens.astype(jnp.float32), norm_gain).astype(jnp.bfloat16)
    offsets = lax.axis_index("sp") * tok_count + jnp.arange(tok_count, dtype=jnp.int32)
    query_latent = jnp.dot(
        normed,
        lax.all_gather(query_down, "sp", axis=0, tiled=True),
        preferred_element_type=jnp.float32,
    )
    value_in = jnp.dot(
        normed,
        lax.all_gather(glu_value, "sp", axis=0, tiled=True),
        preferred_element_type=jnp.float32,
    )
    gate_in = jnp.dot(
        normed,
        lax.all_gather(glu_gate, "sp", axis=0, tiled=True),
        preferred_element_type=jnp.float32,
    )
    latent_query = rms_scale(query_latent, query_gain).astype(jnp.bfloat16)
    query_all = jnp.dot(latent_query, query_up, preferred_element_type=jnp.float32).reshape(
        tok_count, head_count, NOPE + ROPE
    )
    query_plain = query_all[:, :, :NOPE].astype(jnp.bfloat16)
    query_rope = rotate(query_all[:, :, NOPE:], angles_for(offsets, ROPE)[:, None, :]).astype(
        jnp.bfloat16
    )
    absorbed = jnp.einsum(
        "thd,rhd->htr",
        query_plain,
        key_up.reshape(KVR, head_count, NOPE),
        preferred_element_type=jnp.float32,
    ).astype(jnp.bfloat16)
    queries = jnp.concatenate([absorbed, jnp.transpose(query_rope, (1, 0, 2))], axis=-1)
    score_scale = (NOPE + ROPE) ** (-0.5)
    half_rows = tok_count // lax.axis_size("tp")
    first_row = lax.axis_index("tp") * half_rows
    own_rows = lax.dynamic_slice_in_dim(normed, first_row, half_rows, 0)
    own_positions = lax.dynamic_slice_in_dim(offsets, first_row, half_rows, 0)
    own_keys = key_block(own_rows, latent_down, latent_gain, rope_down, own_positions)
    block_keys = lax.all_gather(own_keys, ("sp", "tp"), axis=0, tiled=True)
    row_max = jnp.full((head_count, tok_count), far_below, jnp.float32)
    scores = (
        jnp.einsum("hqc,kc->hqk", queries, block_keys, preferred_element_type=jnp.float32)
        * score_scale
    )
    new_max = jnp.maximum(row_max, jnp.max(scores, axis=2))
    weights = jnp.exp(scores - new_max[:, :, None])
    new_sum = jnp.sum(weights, axis=2)
    added = jnp.einsum(
        "hqk,kr->hqr",
        weights.astype(jnp.bfloat16),
        block_keys[:, :KVR],
        preferred_element_type=jnp.float32,
    )
    gated_rows = (value_in * jax.nn.sigmoid(gate_in)).astype(jnp.bfloat16)
    padded = padded_2(gated_rows, (("sp", 0),), reach_rows)
    filtered = padded[0:tok_count].astype(jnp.float32) * conv_taps[0].astype(jnp.float32)
    for tap_index in range(1, conv_taps.shape[0]):
        filtered = filtered + padded[tap_index : tap_index + tok_count].astype(
            jnp.float32
        ) * conv_taps[tap_index].astype(jnp.float32)
    grouped = filtered.reshape(tok_count, -1, CH // GROUPS)
    centred = grouped - jnp.mean(grouped, axis=-1, keepdims=True)
    spread = jnp.mean(centred * centred, axis=-1, keepdims=True)
    normal_groups = (centred * lax.rsqrt(spread + norm_eps)).reshape(tok_count, -1)
    conv_branch = jax.nn.silu(normal_groups * group_gain.astype(jnp.float32)).astype(jnp.bfloat16)
    attended = (added / new_sum[:, :, None]).astype(jnp.bfloat16)
    log_weight = new_max + jnp.log(new_sum)
    head_out = jnp.einsum(
        "htr,rhv->thv",
        attended,
        value_up.reshape(KVR, head_count, VDIM),
        preferred_element_type=jnp.float32,
    )
    head_out = head_out.reshape(tok_count, head_count * VDIM).astype(jnp.bfloat16)
    mixed_in = jnp.concatenate([head_out, conv_branch], axis=1)
    out_weight = jnp.concatenate([head_proj, channel_proj], axis=0)
    partial_terms = jnp.dot(
        mixed_in,
        lax.all_gather(out_weight, "sp", axis=1, tiled=True),
        preferred_element_type=jnp.float32,
    )
    mixed_out = lax.psum_scatter(
        partial_terms.astype(jnp.bfloat16), "tp", scatter_dimension=1, tiled=True
    )
    return (mixed_out, log_weight)


def solution(mesh):
    in_specs = (
        P(("fs", "sp"), None),
        P(),
        P("sp", None),
        P(),
        P(),
        P(),
        P(),
        P(None, "tp"),
        P(None, "tp"),
        P(None, "tp"),
        P("sp", "tp"),
        P("sp", "tp"),
        P(None, "tp"),
        P("tp"),
        P("tp", "sp"),
        P("tp", "sp"),
    )
    out_specs = (P(("fs", "sp"), "tp"), P("tp", ("fs", "sp")))
    return jax.shard_map(
        per_device, mesh=mesh, in_specs=in_specs, out_specs=out_specs, check_vma=False
    )
```

profile of v0, /device:TPU:0, one launch (start us, length us, event | category | flops | bytes accessed | tf_op | source)
XLA Modules:
  0.0 250.3 jit_solution(11534112967681167767)
XLA Ops:
  7.2 0.7 all-gather.7.cloned.1.call-update
  8.0 0.7 all-gather.9.cloned.1.call-update
  8.7 0.7 all-gather.5.cloned.1.call-update
  9.5 2.2 pad_maximum_fusion
  11.9 0.2 fusion.8
  12.1 0.1 fusion.68
  12.2 0.2 fusion.10
  12.4 0.4 multiply_reduce_fusion.2
  12.8 0.1 broadcast_multiply_fusion.4
  12.9 0.1 copy.32
  13.1 0.1 copy.33
  13.2 0.6 convert_element_type.278
  13.8 0.1 fusion.62
  13.9 0.1 broadcast_multiply_fusion.2
  14.0 0.2 fusion.26
  14.2 0.2 subtract_convert_fusion.1
  14.4 0.1 multiply_convert_fusion.3
  14.5 0.1 pad_maximum_fusion.3
  14.6 17.5 %all_gather.16 = bf16[512,320]{1,0:T(8,128)(2,1)S(1)} all-gather(bf16[64,320]{1,0:T(8,128)(2,1)S(1)} %pad_maximum_fusion.3), channel_id=1, replica_groups=mesh['sp'=4,'fs'=4,'tp'=2] {'sp','tp'}, dimensions={0}, use_global_device_ids=true | all-gather | bytes 368640 | tf_op jit(solution)/shard_map/all_gather | solution.py:123
  32.0 0.6 slice_convert_fusion.31
  32.7 0.7 slice_convert_fusion.32
  33.4 26.5 %all-gather.7.cloned.1.call-done = bf16[2048,512]{1,0:T(8,128)(2,1)} async-done(((bf16[512,512]{1,0:T(8,128)(2,1)}), bf16[2048,512]{1,0:T(8,128)(2,1)}) %all-gather.7.cloned.1.call-update) | async-done | bytes 2097168 | tf_op jit(solution)/shard_map/all_gather | solution.py:94
  59.8 2.0 fusion.75
  61.9 44.5 %all-gather.9.cloned.1.call-done = bf16[2048,512]{1,0:T(8,128)(2,1)} async-done(((bf16[512,512]{1,0:T(8,128)(2,1)}), bf16[2048,512]{1,0:T(8,128)(2,1)}) %all-gather.9.cloned.1.call-update) | async-done | bytes 2097168 | tf_op jit(solution)/shard_map/all_gather | solution.py:99
  106.4 2.1 fusion.6
  108.5 0.6 copy-done.6
  109.1 0.6 fusion.73
  109.7 2.7 %collective-permute-start = (bf16[15,512]{1,0:T(8,128)(2,1)}, bf16[15,512]{1,0:T(8,128)(2,1)}, u32[]{:S(2)}, u32[]{:S(2)}) collective-permute-start(bf16[15,512]{1,0:T(8,128)(2,1)} %get-tuple-element.6), channel_id=1, source_target_pairs={{0,8},{8,16},{16,24},{1,9},{9,17},{17,25},{2,10},{10,18},{18,26},{... | collective-permute-start | bytes 46088 | tf_op jit(solution)/shard_map/ppermute | solution.py:23
  112.4 1.3 collective-permute-start.1
  113.7 38.9 %all-gather.5.cloned.1.call-done = bf16[2048,512]{1,0:T(8,128)(2,1)} async-done(((bf16[512,512]{1,0:T(8,128)(2,1)}), bf16[2048,512]{1,0:T(8,128)(2,1)}) %all-gather.5.cloned.1.call-update) | async-done | bytes 2097168 | tf_op jit(solution)/shard_map/all_gather | solution.py:89
  152.6 2.1 multiply_reduce_fusion.1
  154.8 0.5 fusion.30
  155.3 0.3 convolution_convert_fusion.1
  155.6 0.6 fusion.74
  156.2 0.3 fusion.11
  156.8 0.6 fusion.7
  157.4 0.1 copy.28
  157.9 2.3 multiply_add_fusion
  160.2 0.1 reshape.166
  160.3 0.2 reduce_sum.58
  160.5 0.4 multiply_reduce_fusion
  160.9 0.2 mul.764
  161.1 0.2 sub.45
  161.3 0.1 multiply_convert_fusion
  161.4 72.0 %all-gather.11.cloned.1.call-done = bf16[1024,2048]{1,0:T(8,128)(2,1)} async-done(((bf16[1024,512]{1,0:T(8,128)(2,1)}), bf16[1024,2048]{1,0:T(8,128)(2,1)}) %all-gather.11.cloned.1.call-update) | async-done | bytes 4194320 | tf_op jit(solution)/shard_map/all_gather | solution.py:163
  233.4 3.7 %convolution_convert_fusion = bf16[128,2048]{1,0:T(8,128)(2,1)} fusion(bf16[1024,2048]{1,0:T(8,128)(2,1)} %all-gather.11.cloned.1.call-done, bf16[128,512]{1,0:T(8,128)(2,1)S(1)} %multiply_convert_fusion, bf16[128,512]{1,0:T(8,128)(2,1)S(1)} %copy.28), kind=kOutput, calls=%fused_computation | convolution fusion | flops 537657344 | bytes 4980736 | tf_op jit(solution)/shard_map/dot_general | solution.py:161
  237.2 0.6 log_add_fusion
  237.8 6.0 %reduce-scatter.2.cloned.1.call-done = bf16[128,1024]{1,0:T(8,128)(2,1)} async-done(((bf16[128,2048]{1,0:T(8,128)(2,1)}), bf16[128,1024]{1,0:T(8,128)(2,1)}) %reduce-scatter.2.cloned.1.call-update) | async-done | bytes 262160 | tf_op jit(solution)/shard_map/reduce_scatter | solution.py:166
  (113 shorter events, 0.6 us)
Async XLA Ops:
  7.2 5.2 %copy-start = (bf16[2048,256]{1,0:T(8,128)(2,1)S(1)}, bf16[2048,256]{1,0:T(8,128)(2,1)}, u32[]{:S(2)}) copy-start(bf16[2048,256]{1,0:T(8,128)(2,1)} %param.20) | copy-start | bytes 3145732
  7.2 52.6 %all-gather.7.cloned.1.call-start = ((), (), s32[]{:S(2)}) async-start(), calls=%async_computation.2 | async-start | bytes 2621440 | tf_op jit(solution)/shard_map/all_gather | solution.py:94
  7.9 4.0 %copy-start.41 = (bf16[2048]{0:T(1024)(128)(2,1)S(1)}, bf16[2048]{0:T(1024)(128)(2,1)}, u32[]{:S(2)}) copy-start(bf16[2048]{0:T(1024)(128)(2,1)} %param.17) | copy-start | bytes 12292
  7.9 4.0 %copy-start.1 = (bf16[128,2048]{1,0:T(8,128)(2,1)S(1)}, bf16[128,2048]{1,0:T(8,128)(2,1)}, u32[]{:S(2)}) copy-start(bf16[128,2048]{1,0:T(8,128)(2,1)} %param.16) | copy-start | bytes 1572868
  7.9 98.4 %all-gather.9.cloned.1.call-start = ((), (), s32[]{:S(2)}) async-start(), calls=%async_computation.3 | async-start | bytes 2621440 | tf_op jit(solution)/shard_map/all_gather | solution.py:99
  8.7 143.9 %all-gather.5.cloned.1.call-start = ((), (), s32[]{:S(2)}) async-start(), calls=%async_computation.1 | async-start | bytes 2621440 | tf_op jit(solution)/shard_map/all_gather | solution.py:89
  9.4 224.0 %all-gather.11.cloned.1.call-start = ((), (), s32[]{:S(2)}) async-start(), calls=%async_computation.4 | async-start | bytes 5242880 | tf_op jit(solution)/shard_map/all_gather | solution.py:163
  11.7 1.2 copy-start.44
  11.7 1.2 copy-start.42
  11.7 1.2 copy-start.4
  11.7 1.4 copy-start.5
  11.7 1.5 copy-start.43
  11.7 232.0 %reduce-scatter.2.cloned.1.call-start = ((), (), s32[]{:S(2)}) async-start(), calls=%async_computation.5 | async-start | bytes 786432 | tf_op jit(solution)/shard_map/reduce_scatter | solution.py:166
  11.9 2.1 copy-start.3
  12.4 19.7 %copy-start.8 = (bf16[31,512]{1,0:T(8,128)(2,1)S(1)}, bf16[31,512]{1,0:T(8,128)(2,1)}, u32[]{:S(2)}) copy-start(bf16[31,512]{1,0:T(8,128)(2,1)} %param.28) | copy-start | bytes 95236
  109.1 45.6 %copy-start.2 = (bf16[512,768]{1,0:T(8,128)(2,1)S(1)}, bf16[512,768]{1,0:T(8,128)(2,1)}, u32[]{:S(2)}) copy-start(bf16[512,768]{1,0:T(8,128)(2,1)} %param.23) | copy-start | bytes 2359300
  109.7 47.8 %collective-permute-start = (bf16[15,512]{1,0:T(8,128)(2,1)}, bf16[15,512]{1,0:T(8,128)(2,1)}, u32[]{:S(2)}, u32[]{:S(2)}) collective-permute-start(bf16[15,512]{1,0:T(8,128)(2,1)} %get-tuple-element.6), channel_id=1, source_target_pairs={{0,8},{8,16},{16,24},{1,9},{9,17},{17,25},{2,10},{10,18},{18,26},{... | collective-permute-start | bytes 46088 | tf_op jit(solution)/shard_map/ppermute | solution.py:23
  112.4 45.1 %collective-permute-start.1 = (bf16[15,512]{1,0:T(8,128)(2,1)}, bf16[15,512]{1,0:T(8,128)(2,1)}, u32[]{:S(2)}, u32[]{:S(2)}) collective-permute-start(bf16[15,512]{1,0:T(8,128)(2,1)} %get-tuple-element.7), channel_id=1, source_target_pairs={{8,0},{16,8},{24,16},{9,1},{17,9},{25,17},{10,2},{18,10},{26,18},{... | collective-permute-start | bytes 46088 | tf_op jit(solution)/shard_map/ppermute | solution.py:26
  156.5 1.0 copy-start.7
  156.5 1.0 copy-start.9
  156.5 1.0 copy-start.10
  156.5 1.0 copy-start.11
  156.5 1.0 copy-start.12
  156.6 1.0 copy-start.13
  156.6 1.0 copy-start.14
  156.6 1.0 copy-start.15
  156.6 1.0 copy-start.16
  156.6 1.0 copy-start.17
  156.6 1.0 copy-start.18
  156.6 1.0 copy-start.19
  156.6 1.0 copy-start.20
  156.6 1.0 copy-start.21
  156.6 1.0 copy-start.22
  156.7 1.0 copy-start.23
  156.7 1.0 copy-start.24
  156.7 1.0 copy-start.25
  156.7 1.0 copy-start.26
  156.7 1.0 copy-start.27
  156.7 1.0 copy-start.28
  156.7 1.0 copy-start.29
  156.7 1.0 copy-start.30
  156.7 1.0 copy-start.31
  156.7 1.0 copy-start.32
  156.8 1.0 copy-start.33
  156.8 1.0 copy-start.34
  156.8 1.0 copy-start.35
  156.8 1.0 copy-start.36
  157.4 3.9 %copy-start.40 = (f32[512]{0:T(512)S(1)}, f32[512]{0:T(512)}, u32[]{:S(2)}) copy-start(f32[512]{0:T(512)} %convert_element_type.278) | copy-start | bytes 6148
  (4 other events, 3.7 us)
Sparse Core Ops, SparseCore 0:
  9.6 50.2 all-gather.6
  61.4 44.9 all-gather.8
  107.9 44.6 all-gather.4
  154.0 79.3 all-gather.10
  237.3 6.3 reduce-scatter.1
where the time goes:
time: 251 us; the launch traced here: 250 us
  waiting for transfers between devices  190 us (76%)
  blocking collectives  17.5 us (7%)
  between operations  14.7 us (6%)
  matrix products  12.5 us (5%)
  other arithmetic  9.21 us (4%)
  starting transfers between devices  4.14 us (2%)
    all_gather x1, waiting for transfers between devices, per_device(): lax.all_gather(out_weight, 'sp', axis=1, tiled=True)  72 us
    all_gather x1, waiting for transfers between devices, per_device(): lax.all_gather(glu_gate, 'sp', axis=0, tiled=True)  44.5 us
    all_gather x1, waiting for transfers between devices, per_device(): lax.all_gather(query_down, 'sp', axis=0, tiled=True)  38.9 us
    all_gather x1, waiting for transfers between devices, per_device(): lax.all_gather(glu_value, 'sp', axis=0, tiled=True)  26.5 us
    all_gather x1, blocking collectives, per_device(): block_keys = lax.all_gather(own_keys, ('sp', 'tp'), axis=0, tiled=True)  17.5 us
    reduce_scatter x1, waiting for transfers between devices, per_device(): lax.psum_scatter(partial_terms.astype(jnp.bfloat16), 'tp', scatter_dimens...  5.98 us
  transfers between devices with their start and end apart: 7, of which 5 were waited for; matrix products, arithmetic and copies ran while one was open for 8% of the time, Pallas kernels for 0%

commit v1 on v0

--- a/solution.py
+++ b/solution.py
@@ -13,6 +13,11 @@
 norm_eps = 1e-06
 rope_base = 10000.0
 far_below = -1e30
+
+
+def _perform_roads(frame, mesh_ax):
+    block_next = lax.all_gather(frame, axis_name=mesh_ax)
+    return jnp.concatenate(block_next, axis=1)
 
 
 def padded_2(block, sides, width):
@@ -159,9 +164,7 @@
     mixed_in = jnp.concatenate([head_out, conv_branch], axis=1)
     out_weight = jnp.concatenate([head_proj, channel_proj], axis=0)
     partial_terms = jnp.dot(
-        mixed_in,
-        lax.all_gather(out_weight, "sp", axis=1, tiled=True),
-        preferred_element_type=jnp.float32,
+        mixed_in, _perform_roads(out_weight, "sp"), preferred_element_type=jnp.float32
     )
     mixed_out = lax.psum_scatter(
         partial_terms.astype(jnp.bfloat16), "tp", scatter_dimension=1, tiled=True

time: 251 us -> 259 us (1.032)
  local copies, waits for them, and re-layouts: 2.34 us -> 9.02 us
  waiting for transfers between devices: 190 us -> 187 us
    reshape x1, local copies, waits for them, and re-layouts: 0.14 us -> 6.31 us  [_perform_roads(): return jnp.concatenate(block_next, axis=1)]
where the time goes in v1:
time: 259 us; the launch traced here: 258 us
  waiting for transfers between devices  187 us (72%)
  blocking collectives  17.5 us (7%)
  between operations  14.7 us (6%)
  matrix products  14.2 us (5%)
  other arithmetic  9.3 us (4%)
  local copies, waits for them, and re-layouts  9.02 us (3%)
  starting transfers between devices  6.62 us (3%)
    all_gather x1, waiting for transfers between devices, _perform_roads(): block_next = lax.all_gather(frame, axis_name=mesh_ax)  70.9 us
    all_gather x1, waiting for transfers between devices, per_device(): lax.all_gather(glu_gate, 'sp', axis=0, tiled=True)  45 us
    all_gather x1, waiting for transfers between devices, per_device(): lax.all_gather(query_down, 'sp', axis=0, tiled=True)  36.9 us
    all_gather x1, waiting for transfers between devices, per_device(): lax.all_gather(glu_value, 'sp', axis=0, tiled=True)  25.8 us
    all_gather x1, blocking collectives, per_device(): block_keys = lax.all_gather(own_keys, ('sp', 'tp'), axis=0, tiled=True)  17.5 us
    reshape x1, local copies, waits for them, and re-layouts, _perform_roads(): return jnp.concatenate(block_next, axis=1)  6.31 us
    reduce_scatter x1, waiting for transfers between devices, per_device(): lax.psum_scatter(partial_terms.astype(jnp.bfloat16), 'tp', scatter_dimens...  5.98 us
  transfers between devices with their start and end apart: 7, of which 5 were waited for; matrix products, arithmetic and copies ran while one was open for 8% of the time, Pallas kernels for 0%

profile of v1, /device:TPU:0, one launch (start us, length us, event | category | flops | bytes accessed | tf_op | source)
XLA Modules:
  0.0 258.0 jit_solution(8051273998710876966)
XLA Ops:
  7.2 0.7 all-gather.8.cloned.1.call-update
  8.0 0.7 all-gather.10.cloned.1.call-update
  8.8 0.7 all-gather.6.cloned.1.call-update
  9.5 2.2 pad_maximum_fusion
  11.9 0.2 fusion.8
  12.1 0.5 convert_element_type.278
  12.7 0.8 copy.70
  13.5 0.1 fusion.70
  13.6 0.2 fusion.10
  13.8 0.4 multiply_reduce_fusion.2
  14.4 0.1 copy.59
  14.5 0.1 copy.57
  14.6 0.1 broadcast_multiply_fusion.2
  14.7 0.2 fusion.28
  14.9 0.2 subtract_convert_fusion.1
  15.3 17.5 %all_gather.19 = bf16[512,320]{1,0:T(8,128)(2,1)S(1)} all-gather(bf16[64,320]{1,0:T(8,128)(2,1)S(1)} %pad_maximum_fusion.3), channel_id=1, replica_groups=mesh['sp'=4,'fs'=4,'tp'=2] {'sp','tp'}, dimensions={0}, use_global_device_ids=true | all-gather | bytes 368640 | tf_op jit(solution)/shard_map/all_gather | solution.py:128
  32.8 0.6 slice_convert_fusion.31
  33.5 0.7 slice_convert_fusion.32
  34.1 25.8 %all-gather.8.cloned.1.call-done = bf16[2048,512]{1,0:T(8,128)(2,1)} async-done(((bf16[512,512]{1,0:T(8,128)(2,1)}), bf16[2048,512]{1,0:T(8,128)(2,1)}) %all-gather.8.cloned.1.call-update) | async-done | bytes 2097168 | tf_op jit(solution)/shard_map/all_gather | solution.py:99
  60.0 2.0 fusion.78
  62.0 45.0 %all-gather.10.cloned.1.call-done = bf16[2048,512]{1,0:T(8,128)(2,1)} async-done(((bf16[512,512]{1,0:T(8,128)(2,1)}), bf16[2048,512]{1,0:T(8,128)(2,1)}) %all-gather.10.cloned.1.call-update) | async-done | bytes 2097168 | tf_op jit(solution)/shard_map/all_gather | solution.py:104
  107.0 2.1 fusion.6
  109.1 0.6 fusion.76
  109.7 1.3 collective-permute-start.1
  111.0 5.1 %collective-permute-start = (bf16[15,512]{1,0:T(8,128)(2,1)}, bf16[15,512]{1,0:T(8,128)(2,1)}, u32[]{:S(2)}, u32[]{:S(2)}) collective-permute-start(bf16[15,512]{1,0:T(8,128)(2,1)} %get-tuple-element.8), channel_id=1, source_target_pairs={{0,8},{8,16},{16,24},{1,9},{9,17},{17,25},{2,10},{10,18},{18,26},{... | collective-permute-start | bytes 46088 | tf_op jit(solution)/shard_map/ppermute | solution.py:28
  116.1 36.9 %all-gather.6.cloned.1.call-done = bf16[2048,512]{1,0:T(8,128)(2,1)} async-done(((bf16[512,512]{1,0:T(8,128)(2,1)}), bf16[2048,512]{1,0:T(8,128)(2,1)}) %all-gather.6.cloned.1.call-update) | async-done | bytes 2097168 | tf_op jit(solution)/shard_map/all_gather | solution.py:94
  153.0 2.1 multiply_reduce_fusion.1
  155.2 0.5 fusion.32
  155.7 0.1 copy.72
  155.8 0.1 copy.71
  156.1 0.1 maximum_bitcast_fusion
  156.2 1.2 convolution_convert_fusion.1
  157.4 0.6 fusion.77
  158.0 0.3 fusion.11
  158.6 0.6 fusion.7
  159.2 0.1 copy.64
  159.6 2.3 multiply_add_fusion
  161.9 0.1 reshape.172
  162.0 0.2 reduce_sum.58
  162.2 0.4 multiply_reduce_fusion
  162.6 0.2 mul.764
  162.8 0.2 sub.45
  163.0 0.1 multiply_convert_fusion
  163.2 70.9 %all-gather.12.cloned.1.call-done = bf16[4096,512]{1,0:T(8,128)(2,1)} async-done(((bf16[1024,512]{1,0:T(8,128)(2,1)}), bf16[4096,512]{1,0:T(8,128)(2,1)}) %all-gather.12.cloned.1.call-update) | async-done | bytes 4194320 | tf_op jit(solution)/shard_map/all_gather | solution.py:19
  234.0 6.3 %copy.65 = bf16[1024,4,512]{0,2,1:T(8,128)(2,1)} copy(bf16[1024,4,512]{2,0,1:T(8,128)(2,1)} %bitcast.84) | data formatting | bytes 8388608 | tf_op jit(solution)/shard_map/reshape | solution.py:20
  240.4 4.5 %convolution_convert_fusion = bf16[128,2048]{1,0:T(8,128)(2,1)} fusion(bf16[1024,2048]{0,1:T(8,128)(2,1)} %bitcast.83, bf16[128,512]{1,0:T(8,128)(2,1)S(1)} %multiply_convert_fusion, bf16[128,512]{1,0:T(8,128)(2,1)S(1)} %copy.64), kind=kOutput, calls=%fused_computation | convolution fusion | flops 537657344 | bytes 4980736 | tf_op jit(solution)/shard_map/dot_general | solution.py:166
  244.9 0.6 log_add_fusion
  245.5 6.0 %reduce-scatter.2.cloned.1.call-done = bf16[128,1024]{1,0:T(8,128)(2,1)} async-done(((bf16[128,2048]{1,0:T(8,128)(2,1)}), bf16[128,1024]{1,0:T(8,128)(2,1)}) %reduce-scatter.2.cloned.1.call-update) | async-done | bytes 262160 | tf_op jit(solution)/shard_map/reduce_scatter | solution.py:169
  (114 shorter events, 0.9 us)
Async XLA Ops:
  7.2 6.6 %copy-start = (bf16[2048,256]{1,0:T(8,128)(2,1)S(1)}, bf16[2048,256]{1,0:T(8,128)(2,1)}, u32[]{:S(2)}) copy-start(bf16[2048,256]{1,0:T(8,128)(2,1)} %param.20) | copy-start | bytes 3145732
  7.2 52.8 %all-gather.8.cloned.1.call-start = ((), (), s32[]{:S(2)}) async-start(), calls=%async_computation.2 | async-start | bytes 2621440 | tf_op jit(solution)/shard_map/all_gather | solution.py:99
  7.9 4.0 %copy-start.39 = (bf16[2048]{0:T(1024)(128)(2,1)S(1)}, bf16[2048]{0:T(1024)(128)(2,1)}, u32[]{:S(2)}) copy-start(bf16[2048]{0:T(1024)(128)(2,1)} %param.17) | copy-start | bytes 12292
  7.9 4.0 %copy-start.1 = (bf16[128,2048]{1,0:T(8,128)(2,1)S(1)}, bf16[128,2048]{1,0:T(8,128)(2,1)}, u32[]{:S(2)}) copy-start(bf16[128,2048]{1,0:T(8,128)(2,1)} %param.16) | copy-start | bytes 1572868
  7.9 99.0 %all-gather.10.cloned.1.call-start = ((), (), s32[]{:S(2)}) async-start(), calls=%async_computation.3 | async-start | bytes 2621440 | tf_op jit(solution)/shard_map/all_gather | solution.py:104
  8.7 3.4 %copy-start.40 = (bf16[512]{0:T(512)(128)(2,1)S(1)}, bf16[512]{0:T(512)(128)(2,1)}, u32[]{:S(2)}) copy-start(bf16[512]{0:T(512)(128)(2,1)} %param.29) | copy-start | bytes 3076
  8.7 4.0 %copy-start.4 = (bf16[256,512]{1,0:T(8,128)(2,1)S(1)}, bf16[256,512]{1,0:T(8,128)(2,1)}, u32[]{:S(2)}) copy-start(bf16[256,512]{1,0:T(8,128)(2,1)} %param.25) | copy-start | bytes 786436
  8.7 144.3 %all-gather.6.cloned.1.call-start = ((), (), s32[]{:S(2)}) async-start(), calls=%async_computation.1 | async-start | bytes 2621440 | tf_op jit(solution)/shard_map/all_gather | solution.py:94
  9.4 4.2 %copy-start.42 = (bf16[256]{0:T(256)(128)(2,1)S(1)}, bf16[256]{0:T(256)(128)(2,1)}, u32[]{:S(2)}) copy-start(bf16[256]{0:T(256)(128)(2,1)} %param.21) | copy-start | bytes 1540
  9.4 224.6 %all-gather.12.cloned.1.call-start = ((), (), s32[]{:S(2)}) async-start(), calls=%async_computation.5 | async-start | bytes 5242880 | tf_op jit(solution)/shard_map/all_gather | solution.py:19
  11.7 2.5 copy-start.41
  11.8 2.9 %copy-start.3 = (bf16[2048,64]{0,1:T(8,128)(2,1)S(1)}, bf16[2048,64]{0,1:T(8,128)(2,1)}, u32[]{:S(2)}) copy-start(bf16[2048,64]{0,1:T(8,128)(2,1)} %param.22) | copy-start | bytes 786436
  11.8 239.7 %reduce-scatter.2.cloned.1.call-start = ((), (), s32[]{:S(2)}) async-start(), calls=%async_computation.4 | async-start | bytes 786432 | tf_op jit(solution)/shard_map/reduce_scatter | solution.py:169
  13.5 19.3 %copy-start.6 = (bf16[31,512]{1,0:T(8,128)(2,1)S(1)}, bf16[31,512]{1,0:T(8,128)(2,1)}, u32[]{:S(2)}) copy-start(bf16[31,512]{1,0:T(8,128)(2,1)} %param.28) | copy-start | bytes 95236
  109.1 46.1 %copy-start.2 = (bf16[512,768]{1,0:T(8,128)(2,1)S(1)}, bf16[512,768]{1,0:T(8,128)(2,1)}, u32[]{:S(2)}) copy-start(bf16[512,768]{1,0:T(8,128)(2,1)} %param.23) | copy-start | bytes 2359300
  109.7 49.6 %collective-permute-start.1 = (bf16[15,512]{1,0:T(8,128)(2,1)}, bf16[15,512]{1,0:T(8,128)(2,1)S(1)}, u32[]{:S(2)}, u32[]{:S(2)}) collective-permute-start(bf16[15,512]{1,0:T(8,128)(2,1)} %get-tuple-element.9), channel_id=1, source_target_pairs={{8,0},{16,8},{24,16},{9,1},{17,9},{25,17},{10,2},{18,10},{26,18},{... | collective-permute-start | bytes 46088 | tf_op jit(solution)/shard_map/ppermute | solution.py:31
  111.0 48.4 %collective-permute-start = (bf16[15,512]{1,0:T(8,128)(2,1)}, bf16[15,512]{1,0:T(8,128)(2,1)}, u32[]{:S(2)}, u32[]{:S(2)}) collective-permute-start(bf16[15,512]{1,0:T(8,128)(2,1)} %get-tuple-element.8), channel_id=1, source_target_pairs={{0,8},{8,16},{16,24},{1,9},{9,17},{17,25},{2,10},{10,18},{18,26},{... | collective-permute-start | bytes 46088 | tf_op jit(solution)/shard_map/ppermute | solution.py:28
  156.1 2.6 copy-start.5
  158.3 1.0 copy-start.7
  158.3 1.0 copy-start.8
  158.3 1.0 copy-start.9
  158.3 1.0 copy-start.10
  158.4 1.0 copy-start.11
  158.4 1.0 copy-start.12
  158.4 1.0 copy-start.13
  158.4 1.0 copy-start.14
  158.4 1.0 copy-start.15
  158.4 1.0 copy-start.16
  158.4 1.0 copy-start.17
  158.4 1.0 copy-start.18
  158.4 1.0 copy-start.19
  158.4 1.0 copy-start.20
  158.5 1.0 copy-start.21
  158.5 1.0 copy-start.22
  158.5 1.0 copy-start.23
  158.5 1.0 copy-start.24
  158.5 1.0 copy-start.25
  158.5 1.0 copy-start.26
  158.5 1.0 copy-start.27
  158.5 1.0 copy-start.28
  158.5 1.0 copy-start.29
  158.5 1.0 copy-start.30
  158.6 1.0 copy-start.31
  158.6 1.0 copy-start.32
  158.6 1.0 copy-start.33
  158.6 1.0 copy-start.34
  158.6 1.0 copy-start.35
  159.2 3.9 %copy-start.38 = (f32[512]{0:T(512)S(1)}, f32[512]{0:T(512)}, u32[]{:S(2)}) copy-start(f32[512]{0:T(512)} %convert_element_type.278) | copy-start | bytes 6148
  (2 other events, 2.1 us)
Sparse Core Ops, SparseCore 0:
  9.6 50.3 all-gather.7
  61.5 45.4 all-gather.9
  108.5 44.4 all-gather.5
  154.5 79.5 all-gather.11
  245.0 6.3 reduce-scatter.1
